TPU v7x, 32 devices: a whole 2x2x4 slice. The times are simulated.
32 devices in a mesh: sp: 8 (over z, y), tp: 4 (over x, core).
Axes of the slice: x: 2, y: 2, z: 4, core: 2. Of those that a mesh axis runs over, the one named last changes fastest.
Arguments:
- queries: bfloat16 [6144, 1024], P('sp', 'tp'), may hold values from -6 to 6
- keys: bfloat16 [6144, 1024], P('sp', 'tp'), may hold values from -6 to 6
- values: bfloat16 [6144, 2048], P('sp', 'tp'), may hold values from -6 to 6
- out_gate: bfloat16 [6144, 2048], P('sp', 'tp'), may hold values from -6 to 6
- input_gates: float32 [2, 4, 6144], P(None, 'tp', 'sp'), may hold values from -4 to 300
- forget_gates: float32 [2, 4, 6144], P(None, 'tp', 'sp'), may hold values from -1 to 16
- doc_ids: int32 [6144], P('sp'), may hold values from 0 to 3, never falling along the last dimension, each value on 1 to 3072 neighbouring positions
- head_gain: float32 [2048], P('tp'), may hold values from 0.1 to 1.9
- w_out: bfloat16 [2048, 2048], P('tp'), may hold values from -0.25 to 0.25
- resid: bfloat16 [6144, 2048], P(('sp', 'tp')), may hold values from -30 to 30
- norm_gain: float32 [2048], replicated, may hold values from 0.1 to 1.9
- w_up: bfloat16 [2048, 8192], P('sp', 'tp'), may hold values from -0.125 to 0.125
- w_down: bfloat16 [8192, 2048], P('tp', 'sp'), may hold values from -0.0625 to 0.0625
Outputs:
- layer_out: bfloat16 [6144, 2048], P(('sp', 'tp'))
Inputs may be any that keep to these rules, and one draw needn't show every extreme that they name: `doc_ids`: document numbers never fall along the positions.
All inputs are finite; a program needn't handle non-finite values.
Results may differ from a plain program's by a relative error of at most 0.013.
Values may be sent and summed in bfloat16 or wider, within the bound.
A program may use at most 128 MiB of HBM per device.

v0:
```python
import functools

import jax
import jax.numpy as jnp
from jax import lax
from jax.experimental import pallas as pl
from jax.experimental.pallas import tpu as pltpu
from jax.sharding import PartitionSpec as P


eps = 1e-06
far_low = -1e30
longest_doc = 3072


MESH = pl.DeviceIdType.MESH
bf16 = jnp.bfloat16
f32 = jnp.float32


def dot(a, b):
    return jnp.dot(a, b, preferred_element_type=f32)


class Lines:
    def __init__(self):
        count = lax.axis_size("sp")
        self.pair = 2 if count % 2 == 0 else 1
        self.line = count // self.pair

    def along(self, value, step):
        table = [
            (z * self.pair + y, (z + step) * self.pair + y)
            for z in range(self.line)
            for y in range(self.pair)
            if 0 <= z + step < self.line
        ]
        return lax.ppermute(value, "sp", table)

    def across(self, value, valid):
        table = [
            (z * self.pair + y, z * self.pair + 1 - y)
            for z in range(self.line)
            if valid(z)
            for y in range(self.pair)
        ]
        return lax.ppermute(value, "sp", table)

    def order(self):
        place = lax.axis_index("sp")
        z, y = place // self.pair, place % self.pair
        sources = []
        for k in range(self.line):
            row = (z + self.line - k) % self.line
            sources.append(row * self.pair + y)
            if self.pair == 2:
                sources.append(row * self.pair + 1 - y)
        return jnp.stack(sources)

    def piece(self, source):
        place = lax.axis_index("sp")
        z, y = place // self.pair, place % self.pair
        k = (z + self.line - source // self.pair) % self.line
        return k * self.pair + (y + source) % self.pair

    def gather(self, own):
        n = self.line
        up, down = {}, {}
        up_side, down_side = {}, {}
        two = self.pair == 2
        own_side = self.across(own, lambda z: True) if two else None
        prev_up = prev_down = own
        for k in range(1, n):
            prev_up = up[k] = self.along(prev_up, 1)
            prev_down = down[k] = self.along(prev_down, -1)
            if two:
                up_side[k] = self.across(prev_up, lambda z: z >= k)
                down_side[k] = self.across(prev_down, lambda z: z + k < n)
        groups = [[own] + ([own_side] if two else [])]
        z = lax.axis_index("sp") // self.pair
        for k in range(1, n):
            below = z >= k
            group = [jnp.where(below, up[k], down[n - k])]
            if two:
                group.append(jnp.where(below, up_side[k], down_side[n - k]))
            groups.append(group)
        return groups


class Heads:
    def __init__(self):
        count = lax.axis_size("tp")
        self.core = 2 if count % 2 == 0 else 1
        self.far = count // self.core

    def swap(self, value):
        count = lax.axis_size("tp")
        return lax.ppermute(value, "tp", [(i, i ^ 1) for i in range(count)])

    def shift(self, value, step):
        table = [
            (x * self.core + c, ((x + step) % self.far) * self.core + c)
            for x in range(self.far)
            for c in range(self.core)
        ]
        return lax.ppermute(value, "tp", table)

    def gather(self, own):
        mine = [own] + [self.shift(own, r) for r in range(1, self.far)]
        if self.core == 1:
            return jnp.concatenate(mine)
        return jnp.concatenate(mine + [self.swap(block) for block in mine])

    def reduce(self, near, away):
        total = near.astype(f32)
        if away is not None:
            total = total + self.swap(away).astype(f32)
        out = total[0]
        for r in range(1, self.far):
            out = out + self.shift(total[r].astype(bf16), -r).astype(f32)
        return out


def local_part(scores, values, exponent, keep):
    top = jnp.max(jnp.where(keep, exponent, far_low), axis=1)
    weights = jnp.where(keep, scores * jnp.exp(exponent - top[:, None]), 0.0)
    return top, dot(weights.astype(bf16), values), jnp.sum(weights, axis=1)


def summary(keys, exponent):
    peak = jnp.max(exponent)
    weighted = (keys * jnp.exp(exponent - peak)[:, None]).astype(bf16)
    return weighted, jnp.sum(weighted.astype(f32), axis=0), peak


def split_row(row, width):
    terms, rest = [], row
    for _ in range(3):
        term = lax.reduce_precision(rest, 8, 7)
        rest = rest - term
        terms.append(term.astype(bf16))
    lines = -(-row.shape[0] // width)
    table = jnp.stack([jnp.pad(t, (0, lines * width - t.shape[0])) for t in terms])
    table = table.reshape(3 * lines, width)
    return jnp.pad(table, ((0, -(3 * lines) % 16), (0, 0)))


def join_row(table, size):
    lines = -(-size // table.shape[1])
    terms = table[: 3 * lines].astype(f32).reshape(3, -1)
    return (terms[0] + terms[1] + terms[2])[:size]


def incoming(memory, row, doc_here, sign, reach):
    count = lax.axis_size("sp")
    place = lax.axis_index("sp")
    depth, width = memory.shape
    sent = jnp.concatenate([memory, split_row(row, width)])
    arrived = []
    for d in range(1, min(reach, count - 1) + 1):
        table = [(i, i + sign * d) for i in range(count) if 0 <= i + sign * d < count]
        got = lax.ppermute(sent, "sp", table)
        arrived.append((join_row(got[depth:], row.shape[0]), got[:depth]))
    passed = jnp.zeros((), f32)
    levels, linked = [], []
    for d, (got, _) in enumerate(arrived, 1):
        there = (place >= d) if sign > 0 else (place + d < count)
        joined = there & (got[depth + 2] == doc_here)
        levels.append(jnp.where(joined, got[depth] + passed, far_low))
        linked.append(joined)
        passed = passed + got[depth + 1]
    top = jnp.max(jnp.stack(levels))
    state = jnp.zeros(memory.shape, f32)
    norm = jnp.zeros((depth,), f32)
    for level, joined, (got, mem) in zip(levels, linked, arrived):
        share = jnp.where(joined, jnp.exp(level - top), 0.0)
        state = state + share * mem.astype(f32)
        norm = norm + share * got[:depth]
    return state.astype(bf16), norm, top, linked[0]


def one_head(queries, keys, values, in_gates, forget_pre, doc_pos, reach):
    length, depth = queries.shape
    scale = depth ** (-0.5)
    place = jnp.arange(length)
    logf = jax.nn.log_sigmoid(forget_pre)
    before = place[:, None] >= place[None, :]
    after = place[:, None] <= place[None, :]
    cum_f = jnp.sum(jnp.where(before, logf[0][None, :], 0.0), axis=1)
    cum_b = jnp.sum(jnp.where(after, logf[1][None, :], 0.0), axis=1)
    total_f, total_b = cum_f[length - 1], cum_b[0]
    first, last = doc_pos[0], doc_pos[length - 1]
    weighted_f, norm_f, peak_f = summary(
        keys, jnp.where(doc_pos == last, total_f - cum_f + in_gates[0], far_low)
    )
    weighted_b, norm_b, peak_b = summary(
        keys, jnp.where(doc_pos == first, total_b - cum_b + in_gates[1], far_low)
    )

    def own_state(weighted):
        return lax.dot_general(
            weighted, values, (((0,), (0,)), ((), ())), preferred_element_type=f32
        ).astype(bf16)

    pad = jnp.zeros((125,), f32)
    row_f = jnp.concatenate([norm_f, jnp.stack([peak_f, total_f, last]), pad])
    row_b = jnp.concatenate([norm_b, jnp.stack([peak_b, total_b, first]), pad])
    state_f, norm_in_f, top_f, has_f = incoming(own_state(weighted_f), row_f, first, 1, reach)
    state_b, norm_in_b, top_b, has_b = incoming(own_state(weighted_b), row_b, last, -1, reach)

    scores = (
        lax.dot_general(queries, keys, (((1,), (1,)), ((), ())), preferred_element_type=f32) * scale
    )
    same = doc_pos[:, None] == doc_pos[None, :]
    wide = queries.astype(f32)

    def finish(cum, gate, keep, state, norm_in, top_in, usable):
        exponent = cum[:, None] - cum[None, :] + gate[None, :]
        top, numer, denom = local_part(scores, values, exponent, keep)
        carried = jnp.where(usable, cum + top_in, far_low)
        peak = jnp.maximum(carried, top)
        local = jnp.exp(top - peak)
        inter = jnp.where(usable, jnp.exp(carried - peak), 0.0) * scale
        denom = local * denom + inter * jnp.sum(wide * norm_in[None, :], axis=1)
        under = 1.0 / jnp.maximum(jnp.abs(denom), 1.0)
        return (local * under)[:, None] * numer + (inter * under)[:, None] * dot(queries, state)

    return finish(
        cum_f, in_gates[0], before & same, state_f, norm_in_f, top_f, has_f & (doc_pos == first)
    ) + finish(
        cum_b, in_gates[1], after & same, state_b, norm_in_b, top_b, has_b & (doc_pos == last)
    )


def pack(w_up, w_down):
    wide = w_down.shape[1]
    count = w_up.shape[1] // wide
    tiles = [w_down[i * wide : (i + 1) * wide] for i in range(count)]
    return jnp.concatenate([w_up, jnp.concatenate(tiles, axis=1)])


def unpack(table, wide):
    count = table.shape[1] // wide
    return jnp.concatenate([table[:, i * wide : (i + 1) * wide] for i in range(count)])


def shards(*args):
    return layer(*args)


def layer(
    queries,
    keys,
    values,
    out_gate,
    input_gates,
    forget_gates,
    doc_ids,
    head_gain,
    w_out,
    resid,
    norm_gain,
    w_up,
    w_down,
):
    length = queries.shape[0]
    heads = input_gates.shape[1]
    depth, width = queries.shape[1] // heads, values.shape[1] // heads
    lines, tps = Lines(), Heads()
    rows = resid.shape[0]
    doc_pos = doc_ids.astype(f32)
    reach = -(-longest_doc // length)
    deep_up, wide_down = w_up.shape[0], w_down.shape[1]
    groups = lines.gather(pack(w_up, w_down))
    ups = [[piece[:deep_up] for piece in group] for group in groups]
    downs = [[unpack(piece[deep_up:], wide_down) for piece in group] for group in groups]
    order = lines.order()

    parts = []
    for h in range(heads):
        at_k, at_v = slice(h * depth, (h + 1) * depth), slice(h * width, (h + 1) * width)
        memory = one_head(
            queries[:, at_k],
            keys[:, at_k],
            values[:, at_v],
            input_gates[:, h],
            forget_gates[:, h],
            doc_pos,
            reach,
        )
        normed = memory * lax.rsqrt(jnp.mean(memory * memory, axis=-1, keepdims=True) + eps)
        gate = jax.nn.sigmoid(out_gate[:, at_v].astype(f32))
        parts.append((normed * head_gain[at_v] * gate).astype(bf16))
    readout = parts[0] if heads == 1 else jnp.concatenate(parts, axis=1)

    projected = dot(readout, w_out).astype(bf16).reshape(tps.far, tps.core, rows, -1)
    me = lax.axis_index("tp")
    x, c = me // tps.core, me % tps.core

    def for_core(core):
        picked = lax.dynamic_index_in_dim(projected, core, 1, False)
        return jnp.stack(
            [
                lax.dynamic_index_in_dim(picked, (x + tps.far - r) % tps.far, 0, False)
                for r in range(tps.far)
            ]
        )

    summed = tps.reduce(for_core(c), for_core(1 - c) if tps.core == 2 else None)
    mixed = resid.astype(f32) + summed
    factor = lax.rsqrt(jnp.mean(mixed * mixed, axis=-1, keepdims=True) + eps)
    scaled = (mixed * factor * norm_gain).astype(bf16)

    blocks = order.shape[0]
    deep = scaled.shape[1] // blocks
    turned = jnp.concatenate(
        [lax.dynamic_slice_in_dim(scaled, order[i] * deep, deep, 1) for i in range(blocks)], axis=1
    )
    up_full = jnp.concatenate([piece for group in ups for piece in group], axis=0)
    product = dot(tps.gather(turned), up_full)
    hidden = jnp.square(jax.nn.relu(product)).astype(bf16)

    bundle = max(1, len(downs) // 4)
    outs = []
    for at in range(0, len(downs), bundle):
        pieces = [piece for group in downs[at : at + bundle] for piece in group]
        part = dot(hidden, jnp.concatenate(pieces, axis=1)).astype(bf16)
        part = part.reshape(tps.core, tps.far, rows, -1)
        outs.append(tps.reduce(part[0], part[1] if tps.core == 2 else None))
    summed = jnp.concatenate(outs, axis=1)
    back = jnp.concatenate(
        [lax.dynamic_slice_in_dim(summed, lines.piece(i) * deep, deep, 1) for i in range(blocks)],
        axis=1,
    )
    return (mixed + back).astype(bf16)


class Spot:
    def __init__(self, n_sp, n_tp):
        self.n_sp, self.n_tp = n_sp, n_tp
        self.line = n_sp // 2
        self.sp = lax.axis_index("sp")
        self.tp = lax.axis_index("tp")
        self.z, self.y = self.sp // 2, self.sp % 2
        self.x, self.c = self.tp // 2, self.tp % 2
        self.zp = self.z % 2
        self.base = self.z - self.zp

    def at(self, z=None, y=None, x=None, c=None):
        z = self.z if z is None else z
        y = self.y if y is None else y
        x = self.x if x is None else x
        c = self.c if c is None else c
        return (z * 2 + y, x * 2 + c)


class Wire:
    def __init__(self, send_sems, recv_sems):
        self.send_sems, self.recv_sems = send_sems, recv_sems
        self.count = 0

    def slot(self):
        self.count += 1
        return self.count - 1

    def copy(self, src, dst, number, where, arrival=None):
        return pltpu.make_async_remote_copy(
            src_ref=src,
            dst_ref=dst,
            send_sem=self.send_sems.at[number],
            recv_sem=self.recv_sems.at[number if arrival is None else arrival],
            device_id=where,
            device_id_type=MESH,
        )


def layer_kernel(
    n_sp,
    n_tp,
    q_hbm,
    k_hbm,
    v_hbm,
    og_hbm,
    ig_ref,
    fg_ref,
    doc_ref,
    hg_ref,
    wo_hbm,
    res_hbm,
    ng_ref,
    wup_hbm,
    wdn_hbm,
    out_ref,
    q_s,
    k_s,
    v_s,
    og_s,
    wo_s,
    res_s,
    up_s,
    dn_s,
    rows_s,
    cols_s,
    num_s,
    stat_s,
    own_s,
    own_info_s,
    got_s,
    got_info_s,
    mid_s,
    mid_info_s,
    fin_s,
    proj_s,
    fa_s,
    fb_s,
    fc_s,
    fc_in_s,
    mixed_s,
    nrm_s,
    hid_s,
    part_s,
    r1_s,
    r2_out_s,
    r2_keep_s,
    r2_in_s,
    r3_out_s,
    r3_in_s,
    local_sem,
    send_sem,
    recv_sem,
):
    me = Spot(n_sp, n_tp)
    wire = Wire(send_sem, recv_sem)
    line = me.line
    length, depth = q_s.shape
    rows = res_s.shape[0]
    half = rows // 2
    deep = wup_hbm.shape[0]
    hidden = up_s.shape[2]
    wide = wdn_hbm.shape[1]
    scale = depth ** (-0.5)
    waits = []

    def start(copy, cond=None):
        if cond is None:
            copy.start()
            waits.append((copy, None))
        else:
            pl.when(cond)(copy.start)
            waits.append((copy, cond))

    def load(src, dst, number):
        copy = pltpu.make_async_copy(src, dst, local_sem.at[number])
        copy.start()
        return copy

    up_z = [wire.slot() for _ in range(line)][0]
    dn_z = [wire.slot() for _ in range(line)][0]
    up_y = [wire.slot() for _ in range(line)][0]
    dn_y = [wire.slot() for _ in range(line)][0]

    planes = [me.z, me.base + 1 - me.zp] + [lax.rem(me.base + i, line) for i in range(2, line)]

    def up_piece(z):
        return wup_hbm.at[:, pl.ds(pl.multiple_of((z % 2) * hidden, hidden), hidden)]

    def dn_piece(z):
        return wdn_hbm.at[pl.ds(pl.multiple_of((z % 2) * hidden, hidden), hidden), :]

    def send_up(i):
        z = planes[i]
        start(wire.copy(up_piece(z), up_s.at[me.sp], up_z + z, me.at(z=z), up_z + me.z))

    def send_dn(i):
        z = planes[i]
        start(wire.copy(dn_piece(z), dn_s.at[me.sp], dn_z + z, me.at(z=z), dn_z + me.z))

    def recv_up(z):
        wire.copy(up_piece(z), up_s.at[z * 2 + me.y], up_z + z, me.at(z=z)).wait_recv()

    def recv_dn(z):
        wire.copy(dn_piece(z), dn_s.at[z * 2 + me.y], dn_z + z, me.at(z=z)).wait_recv()

    def cross_up(z, src=None):
        slot = z * 2 + me.y
        src = up_s.at[slot] if src is None else src
        start(wire.copy(src, up_s.at[slot], up_y + z, me.at(y=1 - me.y)))

    def cross_dn(z, src=None):
        slot = z * 2 + me.y
        src = dn_s.at[slot] if src is None else src
        start(wire.copy(src, dn_s.at[slot], dn_y + z, me.at(y=1 - me.y)))

    def crossed_up(z):
        slot = z * 2 + 1 - me.y
        wire.copy(up_s.at[slot], up_s.at[slot], up_y + z, me.at(y=1 - me.y)).wait_recv()

    def crossed_dn(z):
        slot = z * 2 + 1 - me.y
        wire.copy(dn_s.at[slot], dn_s.at[slot], dn_y + z, me.at(y=1 - me.y)).wait_recv()

    for i in range(2, line):
        send_up(i)
    cross_up(me.z, up_piece(me.z))
    k_in = load(k_hbm, k_s, 0)
    v_in = load(v_hbm, v_s, 1)
    q_in = load(q_hbm, q_s, 2)
    og_in = load(og_hbm, og_s, 3)
    wo_in = load(wo_hbm, wo_s, 4)
    res_in = load(res_hbm, res_s, 5)
    up_in = load(up_piece(me.z), up_s.at[me.sp], 6)
    dn_in = load(dn_piece(me.z), dn_s.at[me.sp], 7)

    lane = lax.broadcasted_iota(jnp.int32, (8, length), 1)
    sub = lax.broadcasted_iota(jnp.int32, (8, length), 0)
    pre = fg_ref[...]
    logf = jnp.minimum(pre, 0.0) - jnp.log1p(jnp.exp(-jnp.abs(pre)))
    cum_f = jnp.broadcast_to(logf[0:1], (8, length))
    cum_b = jnp.broadcast_to(logf[1:2], (8, length))
    step = 1
    while step < length:
        cum_f = cum_f + jnp.where(lane >= step, pltpu.roll(cum_f, step, 1), 0.0)
        cum_b = cum_b + jnp.where(lane < length - step, pltpu.roll(cum_b, length - step, 1), 0.0)
        step *= 2
    gate = ig_ref[...]
    rel_f = jnp.broadcast_to(gate[0:1], (8, length)) - cum_f
    rel_b = jnp.broadcast_to(gate[1:2], (8, length)) - cum_b
    doc = jnp.broadcast_to(doc_ref[...].astype(f32), (8, length))
    total_f, total_b = cum_f[:, length - 1 :], cum_b[:, 0:1]
    first, last = doc[:, 0:1], doc[:, length - 1 :]
    exp_f = jnp.where(doc == last, total_f + rel_f, far_low)
    exp_b = jnp.where(doc == first, total_b + rel_b, far_low)
    peak_f = jnp.max(exp_f, axis=1, keepdims=True)
    peak_b = jnp.max(exp_b, axis=1, keepdims=True)
    keep_f, keep_b = jnp.exp(exp_f - peak_f), jnp.exp(exp_b - peak_b)
    rows_s[...] = jnp.where(sub == 0, rel_f, jnp.where(sub == 1, rel_b, doc))
    table = jnp.where(sub == 0, cum_f, cum_b)
    table = jnp.where(sub == 2, doc, table)
    table = jnp.where(sub == 3, keep_f, table)
    table = jnp.where(sub == 4, keep_b, table)
    cols_s[...] = table.T

    k_in.wait()
    v_in.wait()
    wide_keys = k_s[...].astype(f32)

    def own(d, column, peak, total, doc_out):
        weighted = (wide_keys * cols_s[:, column : column + 1]).astype(bf16)
        norm = jnp.sum(weighted.astype(f32), axis=0, keepdims=True)
        own_s[d] = lax.dot_general(
            weighted, v_s[...], (((0,), (0,)), ((), ())), preferred_element_type=f32
        ).astype(bf16)
        at = lax.broadcasted_iota(jnp.int32, (8, depth), 0)
        info = jnp.where(at == 0, jnp.broadcast_to(norm, (8, depth)), peak)
        info = jnp.where(at == 2, total, info)
        own_info_s[d] = jnp.where(at == 3, doc_out, info)

    own(0, 3, peak_f, total_f, last)
    own(1, 4, peak_b, total_b, first)

    def reach_of(d, far):
        sign = 1 if d == 0 else -1
        to, frm = me.sp + sign * far, me.sp - sign * far
        can_send = (to < n_sp) if d == 0 else (to >= 0)
        can_recv = (frm >= 0) if d == 0 else (frm < n_sp)
        return to, can_send, can_recv

    state_no = [[(wire.slot(), wire.slot()) for _ in range(2)] for _ in range(3)]

    def state_copies(r, d, far, src, info):
        to, can_send, can_recv = reach_of(d, far)
        to = jnp.clip(to, 0, n_sp - 1)
        a, b = state_no[r][d]
        return (
            wire.copy(src.at[d], got_s.at[r, d], a, (to, me.tp)),
            wire.copy(info.at[d], got_info_s.at[r, d], b, (to, me.tp)),
            can_send,
            can_recv,
        )

    def state_send(r, d, far, src, info):
        mem, note, can_send, can_recv = state_copies(r, d, far, src, info)
        start(note, can_send)
        start(mem, can_send)

        @pl.when(jnp.logical_not(can_recv))
        def _():
            got_s[r, d] = jnp.zeros(got_s.shape[2:], bf16)
            got_info_s[r, d] = jnp.full(got_info_s.shape[2:], -1.0, f32)

    def state_recv(r, d, far, src, info):
        mem, note, _, can_recv = state_copies(r, d, far, src, info)

        @pl.when(can_recv)
        def _():
            note.wait_recv()
            mem.wait_recv()

    for far in (1, 2):
        for d in (0, 1):
            state_send(far - 1, d, far, own_s, own_info_s)
    send_up(1)

    q_in.wait()

    def inside(j, carry):
        r0 = pl.multiple_of(j * rows, rows)
        score = (
            lax.dot_general(
                q_s[pl.ds(r0, rows), :],
                k_s[...],
                (((1,), (1,)), ((), ())),
                preferred_element_type=f32,
            )
            * scale
        )
        at_row = lax.broadcasted_iota(jnp.int32, (rows, length), 0) + r0
        at_col = lax.broadcasted_iota(jnp.int32, (rows, length), 1)
        cols = cols_s[pl.ds(r0, rows), :]
        same = cols[:, 2:3] == rows_s[2:3, :]
        for d in (0, 1):
            order = (at_row >= at_col) if d == 0 else (at_row <= at_col)
            exponent = jnp.where(
                same & order, cols[:, d : d + 1] + rows_s[d : d + 1, :], far_low
            )
            top = jnp.max(exponent, axis=1, keepdims=True)
            weights = score * jnp.exp(exponent - top)
            stat_s[2 * d, pl.ds(r0, rows), :] = top
            stat_s[2 * d + 1, pl.ds(r0, rows), :] = jnp.sum(weights, axis=1, keepdims=True)
            num_s[d, pl.ds(r0, rows), :] = jnp.dot(
                weights.astype(bf16), v_s[...], preferred_element_type=f32
            )
        return carry

    lax.fori_loop(0, length // rows, inside, 0)

    def info_row(r, d, i):
        return got_info_s[r, d, i : i + 1, :]

    near = []
    for d in (0, 1):
        here = (first if d == 0 else last)[0:1]
        state_recv(0, d, 1, own_s, own_info_s)
        state_recv(1, d, 2, own_s, own_info_s)
        link1 = info_row(0, d, 3) == here
        link2 = info_row(1, d, 3) == here
        level1 = jnp.where(link1, info_row(0, d, 1), far_low)
        level2 = jnp.where(link2, info_row(1, d, 1) + info_row(0, d, 2), far_low)
        top = jnp.maximum(level1, level2)
        share1 = jnp.where(link1, jnp.exp(level1 - top), 0.0)
        share2 = jnp.where(link2, jnp.exp(level2 - top), 0.0)
        norm = share1 * info_row(0, d, 0) + share2 * info_row(1, d, 0)
        mid_s[d] = (
            share1[:, 0:1] * got_s[0, d].astype(f32) + share2[:, 0:1] * got_s[1, d].astype(f32)
        ).astype(bf16)
        at = lax.broadcasted_iota(jnp.int32, (8, depth), 0)
        mid_info_s[d] = jnp.where(at == 0, norm, jnp.where(at == 1, top, here))
        state_send(2, d, 2, mid_s, mid_info_s)
        near.append((here, top, norm))

    for i in range(2, line):
        recv_up(planes[i])
        cross_up(planes[i])
    recv_up(planes[1])
    cross_up(planes[1])

    ends = []
    for d in (0, 1):
        here, top, norm = near[d]
        state_recv(2, d, 2, mid_s, mid_info_s)
        link = info_row(2, d, 3) == here
        level = jnp.where(
            link, info_row(2, d, 1) + info_row(1, d, 2) + info_row(0, d, 2), far_low
        )
        peak = jnp.maximum(top, level)
        link1 = info_row(0, d, 3) == here
        share = jnp.where(link1, jnp.exp(top - peak), 0.0)
        share_far = jnp.where(link, jnp.exp(level - peak), 0.0)
        fin_s[d] = (
            share[:, 0:1] * mid_s[d].astype(f32) + share_far[:, 0:1] * got_s[2, d].astype(f32)
        ).astype(bf16)
        meets = jnp.where(link1, here, -2.0)
        ends.append((meets[:, 0:1], peak, share * norm + share_far * info_row(2, d, 0)))

    og_in.wait()
    wo_in.wait()

    def project(j, store):
        r0 = pl.multiple_of(j * rows, rows)
        queries = q_s[pl.ds(r0, rows), :]
        wide_q = queries.astype(f32)
        cols = cols_s[pl.ds(r0, rows), :]
        memory = None
        for d in (0, 1):
            meets, level, norm = ends[d]
            usable = cols[:, 2:3] == meets
            carried = jnp.where(usable, cols[:, d : d + 1] + level[:, 0:1], far_low)
            top = stat_s[2 * d, pl.ds(r0, rows), :]
            peak = jnp.maximum(carried, top)
            local = jnp.exp(top - peak)
            inter = jnp.where(usable, jnp.exp(carried - peak), 0.0) * scale
            den = local * stat_s[2 * d + 1, pl.ds(r0, rows), :] + inter * jnp.sum(
                wide_q * norm, axis=1, keepdims=True
            )
            under = 1.0 / jnp.maximum(jnp.abs(den), 1.0)
            term = (local * under) * num_s[d, pl.ds(r0, rows), :] + (inter * under) * jnp.dot(
                queries, fin_s[d], preferred_element_type=f32
            )
            memory = term if memory is None else memory + term
        normed = memory * lax.rsqrt(jnp.mean(memory * memory, axis=1, keepdims=True) + eps)
        open_gate = jax.nn.sigmoid(og_s[pl.ds(r0, rows), :].astype(f32))
        readout = (normed * hg_ref[...] * open_gate).astype(bf16)
        store(jnp.dot(readout, wo_s[...], preferred_element_type=f32))

    fa_no, fb_no, fc_no = wire.slot(), wire.slot(), wire.slot()
    core = me.at(c=1 - me.c)
    over = me.at(x=1 - me.x)
    above = me.at(z=me.base + 1 - me.zp)
    far_x, far_c = 1 - me.x, 1 - me.c

    def put(ref):
        def store(value):
            ref[...] = value.astype(ref.dtype)

        return store

    fa = wire.copy(proj_s.at[0], fa_s, fa_no, core)
    fb = wire.copy(proj_s.at[2], fb_s, fb_no, core)
    fc = wire.copy(fc_s, fc_in_s, fc_no, over)
    project(far_x * 2 + far_c, put(proj_s.at[0]))
    start(fa)
    project(far_x * 2 + me.c, put(proj_s.at[1]))
    fa.wait_recv()
    fc_s[...] = (proj_s[1].astype(f32) + fa_s[...].astype(f32)).astype(bf16)
    start(fc)
    project(me.x * 2 + far_c, put(proj_s.at[2]))
    start(fb)
    project(me.x * 2 + me.c, put(proj_s.at[3]))
    res_in.wait()
    fb.wait_recv()
    near_sum = res_s[...].astype(f32) + proj_s[3].astype(f32) + fb_s[...].astype(f32)
    mixed_s[...] = near_sum
    fc.wait_recv()
    mixed = mixed_s[...] + fc_in_s[...].astype(f32)
    mixed_s[...] = mixed
    factor = lax.rsqrt(jnp.mean(mixed * mixed, axis=1, keepdims=True) + eps)
    mine = me.zp * n_tp + me.tp
    nrm_s[mine] = (mixed * factor * ng_ref[...]).astype(bf16)

    def owner(zp, x, c):
        return zp * n_tp + x * 2 + c

    far_z = 1 - me.zp
    n_core = [wire.slot() for _ in range(5)]
    n_x, n_z, n_xh, n_zh = wire.slot(), wire.slot(), wire.slot(), wire.slot()
    top_half, low_half = pl.ds(0, half), pl.ds(half, half)

    def pass_on(number, where, who, part=None):
        ref = nrm_s.at[who] if part is None else nrm_s.at[who, part]
        return wire.copy(ref, ref, number, where)

    start(pass_on(n_x, over, mine))
    start(pass_on(n_z, above, mine))
    start(pass_on(n_core[0], core, mine))
    for i in range(2, line):
        send_dn(i)
    send_dn(1)
    cross_dn(me.z, dn_piece(me.z))

    up_in.wait()
    for z in planes:
        crossed_up(z)

    def raise_rows(zp, x):
        group = zp * 2 + x

        def chunk(n, carry):
            c0 = pl.multiple_of(n * 256, 256)
            left = nrm_s[pl.ds(group * 2, 2), :, :].reshape(2 * rows, nrm_s.shape[2])
            right = up_s[:, :, pl.ds(c0, 256)].reshape(n_sp * deep, 256)
            pre = jnp.maximum(jnp.dot(left, right, preferred_element_type=f32), 0.0)
            hid_s[group, :, pl.ds(c0, 256)] = (pre * pre).astype(bf16)
            return carry

        lax.fori_loop(0, hidden // 256, chunk, 0)

    pass_on(n_core[0], core, owner(me.zp, me.x, far_c)).wait_recv()
    raise_rows(me.zp, me.x)
    who = owner(me.zp, far_x, me.c)
    pass_on(n_x, over, who).wait_recv()
    start(pass_on(n_zh, above, who, top_half))
    start(pass_on(n_core[1], core, who))
    who = owner(far_z, me.x, me.c)
    pass_on(n_z, above, who).wait_recv()
    start(pass_on(n_xh, over, who, low_half))
    start(pass_on(n_core[2], core, who))
    pass_on(n_core[1], core, owner(me.zp, far_x, far_c)).wait_recv()
    raise_rows(me.zp, far_x)
    pass_on(n_core[2], core, owner(far_z, me.x, far_c)).wait_recv()
    raise_rows(far_z, me.x)
    who = owner(far_z, far_x, me.c)
    pass_on(n_zh, above, who, top_half).wait_recv()
    start(pass_on(n_core[3], core, who, top_half))
    pass_on(n_xh, over, who, low_half).wait_recv()
    start(pass_on(n_core[4], core, who, low_half))
    who = owner(far_z, far_x, far_c)
    pass_on(n_core[3], core, who, top_half).wait_recv()
    pass_on(n_core[4], core, who, low_half).wait_recv()
    raise_rows(far_z, far_x)

    blocks = n_sp
    order = []
    for i in range(line):
        z = lax.rem(me.base + i, line)
        order += [(z, me.y), (z, 1 - me.y)]
    r1_no = [wire.slot() for _ in range(blocks)]
    r2_no = [wire.slot() for _ in range(blocks)]
    r3_no = [wire.slot() for _ in range(blocks)]
    groups = 4

    def pump(i):
        z = lax.rem(me.base + i, line)

        @pl.when(z == me.z)
        def _():
            dn_in.wait()

        if i < 2:

            @pl.when(z != me.z)
            def _():
                recv_dn(z)
                wire.copy(
                    dn_s.at[z * 2 + me.y], dn_s.at[z * 2 + me.y], dn_y + z, me.at(y=1 - me.y)
                ).start()

            waits.append(
                (
                    wire.copy(
                        dn_s.at[z * 2 + me.y], dn_s.at[z * 2 + me.y], dn_y + z, me.at(y=1 - me.y)
                    ),
                    z != me.z,
                )
            )
        else:
            recv_dn(z)
            cross_dn(z)

    def lower(k):
        z, y = order[k]
        if k % 2 == 0:
            if k == 0:
                pump(0)
            if k // 2 + 1 < line:
                pump(k // 2 + 1)
        else:
            crossed_dn(z)
        slot = z * 2 + y

        def one(g, carry):
            value = jnp.dot(hid_s[g], dn_s[slot], preferred_element_type=f32).astype(bf16)
            part_s[k, 0, g] = value[:rows]
            part_s[k, 1, g] = value[rows:]
            return carry

        lax.fori_loop(0, groups, one, 0)
        start(wire.copy(part_s.at[k, far_c], r1_s.at[k], r1_no[k], core))

    def sum1(k):
        wire.copy(part_s.at[k, far_c], r1_s.at[k], r1_no[k], core).wait_recv()

        def both(g):
            return part_s[k, me.c, g].astype(f32) + r1_s[k, g].astype(f32)

        for i in range(2):
            away = i * 2 + far_x if k % 2 == 0 else far_z * 2 + i
            r2_out_s[k, i] = both(away).astype(bf16)
        start(wire.copy(r2_out_s.at[k], r2_in_s.at[k], r2_no[k], over if k % 2 == 0 else above))
        for i in range(2):
            here = i * 2 + me.x if k % 2 == 0 else me.zp * 2 + i
            r2_keep_s[k, i] = both(here)

    def sum2(k):
        wire.copy(
            r2_out_s.at[k], r2_in_s.at[k], r2_no[k], over if k % 2 == 0 else above
        ).wait_recv()
        far = far_z if k % 2 == 0 else far_x
        r3_out_s[k] = (r2_keep_s[k, far] + r2_in_s[k, far].astype(f32)).astype(bf16)
        start(wire.copy(r3_out_s.at[k], r3_in_s.at[k], r3_no[k], above if k % 2 == 0 else over))

    def sum3(k):
        wire.copy(
            r3_out_s.at[k], r3_in_s.at[k], r3_no[k], above if k % 2 == 0 else over
        ).wait_recv()
        z, y = order[k]
        c0 = pl.multiple_of((z * 2 + y) * wide, wide)
        at = me.zp if k % 2 == 0 else me.x
        total = r2_keep_s[k, at] + r2_in_s[k, at].astype(f32) + r3_in_s[k].astype(f32)
        total = mixed_s[:, pl.ds(c0, wide)] + total
        out_ref[:, pl.ds(c0, wide)] = total.astype(bf16)

    for k in range(blocks + 3):
        if k < blocks:
            lower(k)
        if 0 <= k - 1 < blocks:
            sum1(k - 1)
        if 0 <= k - 2 < blocks:
            sum2(k - 2)
        if 0 <= k - 3 < blocks:
            sum3(k - 3)

    for copy, cond in waits:
        if cond is None:
            copy.wait_send()
        else:
            pl.when(cond)(copy.wait_send)


def fused(n_sp, n_tp, *args):
    (
        queries,
        keys,
        values,
        out_gate,
        input_gates,
        forget_gates,
        doc_ids,
        head_gain,
        w_out,
        resid,
        norm_gain,
        w_up,
        w_down,
    ) = args
    length, depth = queries.shape
    width = values.shape[1]
    rows, model = resid.shape
    deep, wide = w_up.shape[0], w_down.shape[1]
    hidden = w_up.shape[1] // 2
    line = n_sp // 2
    blocks = n_sp
    numbers = 4 * line + 24 + 3 * blocks
    vmem = pltpu.VMEM
    scratch = [
        vmem((length, depth), bf16),
        vmem((length, depth), bf16),
        vmem((length, width), bf16),
        vmem((length, width), bf16),
        vmem((width, model), bf16),
        vmem((rows, model), bf16),
        vmem((n_sp, deep, hidden), bf16),
        vmem((n_sp, hidden, wide), bf16),
        vmem((8, length), f32),
        vmem((length, 8), f32),
        vmem((2, length, width), f32),
        vmem((4, length, 1), f32),
        vmem((2, depth, width), bf16),
        vmem((2, 8, depth), f32),
        vmem((3, 2, depth, width), bf16),
        vmem((3, 2, 8, depth), f32),
        vmem((2, depth, width), bf16),
        vmem((2, 8, depth), f32),
        vmem((2, depth, width), bf16),
        vmem((4, rows, model), bf16),
        vmem((rows, model), bf16),
        vmem((rows, model), bf16),
        vmem((rows, model), bf16),
        vmem((rows, model), bf16),
        vmem((rows, model), f32),
        vmem((2 * n_tp, rows, model), bf16),
        vmem((4, 2 * rows, hidden), bf16),
        vmem((blocks, 2, 4, rows, wide), bf16),
        vmem((blocks, 4, rows, wide), bf16),
        vmem((blocks, 2, rows, wide), bf16),
        vmem((blocks, 2, rows, wide), f32),
        vmem((blocks, 2, rows, wide), bf16),
        vmem((blocks, rows, wide), bf16),
        vmem((blocks, rows, wide), bf16),
        pltpu.SemaphoreType.DMA((8,)),
        pltpu.SemaphoreType.DMA((numbers,)),
        pltpu.SemaphoreType.DMA((numbers,)),
    ]
    anywhere = pl.BlockSpec(memory_space=pl.ANY)
    inside = pl.BlockSpec(memory_space=pltpu.VMEM)
    return pl.pallas_call(
        functools.partial(layer_kernel, n_sp, n_tp),
        out_shape=jax.ShapeDtypeStruct((rows, model), bf16),
        in_specs=[anywhere] * 4 + [inside] * 4 + [anywhere] * 2 + [inside] + [anywhere] * 2,
        out_specs=inside,
        scratch_shapes=scratch,
        compiler_params=pltpu.CompilerParams(has_side_effects=True, vmem_limit_bytes=66_000_000),
        name="layer",
    )(
        queries,
        keys,
        values,
        out_gate,
        input_gates.reshape(2, length),
        forget_gates.reshape(2, length),
        doc_ids.reshape(1, length),
        head_gain.reshape(1, width),
        w_out,
        resid,
        norm_gain.reshape(1, model),
        w_up,
        w_down,
    )


def fits(mesh, args):
    n_sp, n_tp = mesh.shape["sp"], mesh.shape["tp"]
    queries, input_gates, w_up, w_down = args[0], args[4], args[11], args[12]
    length = queries.shape[0] // n_sp
    return (
        n_tp == 4
        and n_sp % 4 == 0
        and input_gates.shape[1] == n_tp
        and -(-longest_doc // length) <= 4
        and length % (n_tp * 32) == 0
        and w_down.shape[1] % (n_sp * 128) == 0
        and w_up.shape[0] % (n_sp * 16) == 0
        and w_up.shape[1] % (n_tp * 512) == 0
    )


def solution(mesh):
    in_specs = (
        P("sp", "tp"),
        P("sp", "tp"),
        P("sp", "tp"),
        P("sp", "tp"),
        P(None, "tp", "sp"),
        P(None, "tp", "sp"),
        P("sp"),
        P("tp"),
        P("tp", None),
        P(("sp", "tp"), None),
        P(),
        P("sp", "tp"),
        P("tp", "sp"),
    )
    out_specs = P(("sp", "tp"), None)

    def step(*args):
        whole = fits(mesh, args)
        body = functools.partial(fused, mesh.shape["sp"], mesh.shape["tp"]) if whole else shards
        return jax.shard_map(
            body, mesh=mesh, in_specs=in_specs, out_specs=out_specs, check_vma=False
        )(*args)

    return step
```

profile of v0, /device:TPU:0, one launch (start us, length us, event | category | flops | bytes accessed | tf_op | source)
XLA Modules:
  0.0 224.3 jit_solution(2746970640474762442)
XLA Ops:
  0.0 1.3 reshape.17.doc_ref
  1.3 1.3 copy_bitcast_fusion
  2.6 219.6 %layer.1 = bf16[192,2048]{1,0:T(8,128)(2,1)} custom-call(bf16[768,256]{1,0:T(8,128)(2,1)} %q_hbm.1, bf16[768,256]{1,0:T(8,128)(2,1)} %k_hbm.1, bf16[768,512]{1,0:T(8,128)(2,1)} %v_hbm.1, bf16[768,512]{1,0:T(8,128)(2,1)} %og_hbm.1, f32[2,768]{1,0:T(2,128)} %get-tuple-element.6.ig_ref, f32[2,768]{1,0:T(2,128)} %get-tuple-element.5.fg_ref, ...), custom_call_target="tpu_custom_call" | custom-call | tf_op jit(solution)/shard_map/layer/pallas_call | solution.py:985
  222.2 2.1 copy.19
where the time goes:
time: 225 us; the launch traced here: 224 us
  Pallas kernels  220 us (98%)
  local copies, waits for them, and re-layouts  4.66 us (2%)
    pallas_call x1, Pallas kernels, fused(): pl.pallas_call(functools.partial(layer_kernel, n_sp, n_tp), out_shape=jax...  220 us

commit v1 on v0

--- a/solution.py
+++ b/solution.py
@@ -410,11 +410,8 @@
     mid_s,
     mid_info_s,
     fin_s,
-    proj_s,
-    fa_s,
-    fb_s,
-    fc_s,
-    fc_in_s,
+    read_s,
+    heads_s,
     mixed_s,
     nrm_s,
     hid_s,
@@ -433,8 +430,8 @@
     wire = Wire(send_sem, recv_sem)
     line = me.line
     length, depth = q_s.shape
+    width = v_s.shape[1]
     rows = res_s.shape[0]
-    half = rows // 2
     deep = wup_hbm.shape[0]
     hidden = up_s.shape[2]
     wide = wdn_hbm.shape[1]
@@ -449,71 +446,106 @@
             pl.when(cond)(copy.start)
             waits.append((copy, cond))
 
+    def drain(copy):
+        copy.wait_send()
+        waits[:] = [item for item in waits if item[0] is not copy]
+
     def load(src, dst, number):
         copy = pltpu.make_async_copy(src, dst, local_sem.at[number])
         copy.start()
         return copy
 
-    up_z = [wire.slot() for _ in range(line)][0]
-    dn_z = [wire.slot() for _ in range(line)][0]
-    up_y = [wire.slot() for _ in range(line)][0]
-    dn_y = [wire.slot() for _ in range(line)][0]
-
-    planes = [me.z, me.base + 1 - me.zp] + [lax.rem(me.base + i, line) for i in range(2, line)]
-
-    def up_piece(z):
-        return wup_hbm.at[:, pl.ds(pl.multiple_of((z % 2) * hidden, hidden), hidden)]
-
-    def dn_piece(z):
-        return wdn_hbm.at[pl.ds(pl.multiple_of((z % 2) * hidden, hidden), hidden), :]
-
-    def send_up(i):
-        z = planes[i]
-        start(wire.copy(up_piece(z), up_s.at[me.sp], up_z + z, me.at(z=z), up_z + me.z))
-
-    def send_dn(i):
-        z = planes[i]
-        start(wire.copy(dn_piece(z), dn_s.at[me.sp], dn_z + z, me.at(z=z), dn_z + me.z))
-
-    def recv_up(z):
-        wire.copy(up_piece(z), up_s.at[z * 2 + me.y], up_z + z, me.at(z=z)).wait_recv()
-
-    def recv_dn(z):
-        wire.copy(dn_piece(z), dn_s.at[z * 2 + me.y], dn_z + z, me.at(z=z)).wait_recv()
-
-    def cross_up(z, src=None):
-        slot = z * 2 + me.y
-        src = up_s.at[slot] if src is None else src
-        start(wire.copy(src, up_s.at[slot], up_y + z, me.at(y=1 - me.y)))
-
-    def cross_dn(z, src=None):
-        slot = z * 2 + me.y
-        src = dn_s.at[slot] if src is None else src
-        start(wire.copy(src, dn_s.at[slot], dn_y + z, me.at(y=1 - me.y)))
-
-    def crossed_up(z):
-        slot = z * 2 + 1 - me.y
-        wire.copy(up_s.at[slot], up_s.at[slot], up_y + z, me.at(y=1 - me.y)).wait_recv()
-
-    def crossed_dn(z):
-        slot = z * 2 + 1 - me.y
-        wire.copy(dn_s.at[slot], dn_s.at[slot], dn_y + z, me.at(y=1 - me.y)).wait_recv()
-
-    for i in range(2, line):
-        send_up(i)
-    cross_up(me.z, up_piece(me.z))
+    up_z = [[wire.slot() for _ in range(line)][0] for _ in range(2)]
+    dn_z = [[wire.slot() for _ in range(line)][0] for _ in range(2)]
+    up_y = [[wire.slot() for _ in range(line)][0] for _ in range(2)]
+    dn_y = [[wire.slot() for _ in range(line)][0] for _ in range(2)]
+    ends_line = (me.z == 0) | (me.z == line - 1)
+    inner_line = jnp.logical_not(ends_line)
+
+    planes = [me.z, me.base + 1 - me.zp]
+    for i in range(2, line, 2):
+        pair = lax.rem(me.base + i, line)
+        planes += [pair + me.zp, pair + 1 - me.zp]
+    up_part = [pl.ds(h * (deep // 2), deep // 2) for h in range(2)]
+    dn_part = [pl.ds(h * (hidden // 2), hidden // 2) for h in range(2)]
+
+    def up_piece(z, h):
+        lanes = pl.ds(pl.multiple_of((z % 2) * hidden, hidden), hidden)
+        return wup_hbm.at[up_part[h], lanes]
+
+    def dn_piece(z, h):
+        at = (z % 2) * hidden + h * (hidden // 2)
+        return wdn_hbm.at[pl.ds(pl.multiple_of(at, hidden // 2), hidden // 2), :]
+
+    def send_up(z, h, cond=None):
+        dst = up_s.at[me.sp, up_part[h]]
+        start(wire.copy(up_piece(z, h), dst, up_z[h] + z, me.at(z=z), up_z[h] + me.z), cond)
+
+    def send_dn(z, h, cond=None):
+        dst = dn_s.at[me.sp, dn_part[h]]
+        copy = wire.copy(dn_piece(z, h), dst, dn_z[h] + z, me.at(z=z), dn_z[h] + me.z)
+        start(copy, cond)
+        return copy
+
+    beside = me.at(y=1 - me.y)
+
+    def over_up(z, h, own=False):
+        ref = up_s.at[z * 2 + me.y, up_part[h]]
+        return wire.copy(up_piece(z, h) if own else ref, ref, up_y[h] + z, beside)
+
+    def over_dn(z, h, own=False):
+        ref = dn_s.at[z * 2 + me.y, dn_part[h]]
+        return wire.copy(dn_piece(z, h) if own else ref, ref, dn_y[h] + z, beside)
+
+    def relay_up(z, h):
+        ref = up_s.at[z * 2 + me.y, up_part[h]]
+        wire.copy(ref, ref, up_z[h] + z, me.at(z=z)).wait_recv()
+        start(over_up(z, h))
+
+    def crossed_up(z, h):
+        ref = up_s.at[z * 2 + 1 - me.y, up_part[h]]
+        wire.copy(ref, ref, up_y[h] + z, beside).wait_recv()
+
+    def crossed_dn(z, h):
+        ref = dn_s.at[z * 2 + 1 - me.y, dn_part[h]]
+        wire.copy(ref, ref, dn_y[h] + z, beside).wait_recv()
+
     k_in = load(k_hbm, k_s, 0)
     v_in = load(v_hbm, v_s, 1)
     q_in = load(q_hbm, q_s, 2)
     og_in = load(og_hbm, og_s, 3)
-    wo_in = load(wo_hbm, wo_s, 4)
+    wo_in = load(wo_hbm, wo_s.at[me.tp], 4)
     res_in = load(res_hbm, res_s, 5)
-    up_in = load(up_piece(me.z), up_s.at[me.sp], 6)
-    dn_in = load(dn_piece(me.z), dn_s.at[me.sp], 7)
-
+    own_in = []
+    for h in range(2):
+        own_in.append(load(up_piece(me.z, h), up_s.at[me.sp, up_part[h]], 6 + h))
+    dn_in = [load(dn_piece(me.z, h), dn_s.at[me.sp, dn_part[h]], 8 + h) for h in range(2)]
+
+    barrier = pltpu.get_barrier_semaphore()
+    met = [me.at(z=z) for z in planes[1:]]
+    met += [beside, me.at(c=1 - me.c), me.at(x=1 - me.x), me.at(x=1 - me.x, c=1 - me.c)]
+    met += [(lax.rem(me.sp + i, n_sp), me.tp) for i in (1, n_sp - 1)]
+    for where in met:
+        pl.semaphore_signal(barrier, inc=1, device_id=where, device_id_type=MESH)
+    pl.semaphore_wait(barrier, len(met))
+    send_up(planes[2], 0)
+    send_up(planes[1], 0)
+    start(over_up(me.z, 0, True))
+    wo_no = [wire.slot() for _ in range(3)]
+    core = me.at(c=1 - me.c)
+    over = me.at(x=1 - me.x)
+    above = me.at(z=me.base + 1 - me.zp)
+    far_x, far_c = 1 - me.x, 1 - me.c
+
+    def heads_row(number, where, owner_tp, src=None):
+        ref = wo_s.at[owner_tp]
+        return wire.copy(ref if src is None else src, ref, number, where)
+
+    start(heads_row(wo_no[0], over, me.tp, wo_hbm))
+    start(heads_row(wo_no[1], core, me.tp, wo_hbm))
     lane = lax.broadcasted_iota(jnp.int32, (8, length), 1)
     sub = lax.broadcasted_iota(jnp.int32, (8, length), 0)
-    pre = fg_ref[...]
+    pre = jnp.concatenate([fg_ref[0], fg_ref[1]], axis=0)
     logf = jnp.minimum(pre, 0.0) - jnp.log1p(jnp.exp(-jnp.abs(pre)))
     cum_f = jnp.broadcast_to(logf[0:1], (8, length))
     cum_b = jnp.broadcast_to(logf[1:2], (8, length))
@@ -522,10 +554,10 @@
         cum_f = cum_f + jnp.where(lane >= step, pltpu.roll(cum_f, step, 1), 0.0)
         cum_b = cum_b + jnp.where(lane < length - step, pltpu.roll(cum_b, length - step, 1), 0.0)
         step *= 2
-    gate = ig_ref[...]
+    gate = jnp.concatenate([ig_ref[0], ig_ref[1]], axis=0)
     rel_f = jnp.broadcast_to(gate[0:1], (8, length)) - cum_f
     rel_b = jnp.broadcast_to(gate[1:2], (8, length)) - cum_b
-    doc = jnp.broadcast_to(doc_ref[...].astype(f32), (8, length))
+    doc = jnp.broadcast_to(doc_ref[...].reshape(1, length).astype(f32), (8, length))
     total_f, total_b = cum_f[:, length - 1 :], cum_b[:, 0:1]
     first, last = doc[:, 0:1], doc[:, length - 1 :]
     exp_f = jnp.where(doc == last, total_f + rel_f, far_low)
@@ -599,7 +631,9 @@
     for far in (1, 2):
         for d in (0, 1):
             state_send(far - 1, d, far, own_s, own_info_s)
-    send_up(1)
+    send_up(planes[2], 1)
+    send_up(planes[1], 1)
+    start(over_up(me.z, 1, True))
 
     q_in.wait()
 
@@ -658,11 +692,8 @@
         state_send(2, d, 2, mid_s, mid_info_s)
         near.append((here, top, norm))
 
-    for i in range(2, line):
-        recv_up(planes[i])
-        cross_up(planes[i])
-    recv_up(planes[1])
-    cross_up(planes[1])
+    relay_up(planes[2], 0)
+    relay_up(planes[1], 0)
 
     ends = []
     for d in (0, 1):
@@ -682,10 +713,13 @@
         meets = jnp.where(link1, here, -2.0)
         ends.append((meets[:, 0:1], peak, share * norm + share_far * info_row(2, d, 0)))
 
+    for h in range(2):
+        for i in range(3, line):
+            send_up(planes[i], h)
+    send_dn(planes[2], 0)
     og_in.wait()
-    wo_in.wait()
-
-    def project(j, store):
+
+    def project(j):
         r0 = pl.multiple_of(j * rows, rows)
         queries = q_s[pl.ds(r0, rows), :]
         wide_q = queries.astype(f32)
@@ -709,51 +743,71 @@
             memory = term if memory is None else memory + term
         normed = memory * lax.rsqrt(jnp.mean(memory * memory, axis=1, keepdims=True) + eps)
         open_gate = jax.nn.sigmoid(og_s[pl.ds(r0, rows), :].astype(f32))
-        readout = (normed * hg_ref[...] * open_gate).astype(bf16)
-        store(jnp.dot(readout, wo_s[...], preferred_element_type=f32))
-
-    fa_no, fb_no, fc_no = wire.slot(), wire.slot(), wire.slot()
-    core = me.at(c=1 - me.c)
-    over = me.at(x=1 - me.x)
-    above = me.at(z=me.base + 1 - me.zp)
-    far_x, far_c = 1 - me.x, 1 - me.c
-
-    def put(ref):
-        def store(value):
-            ref[...] = value.astype(ref.dtype)
-
-        return store
-
-    fa = wire.copy(proj_s.at[0], fa_s, fa_no, core)
-    fb = wire.copy(proj_s.at[2], fb_s, fb_no, core)
-    fc = wire.copy(fc_s, fc_in_s, fc_no, over)
-    project(far_x * 2 + far_c, put(proj_s.at[0]))
-    start(fa)
-    project(far_x * 2 + me.c, put(proj_s.at[1]))
-    fa.wait_recv()
-    fc_s[...] = (proj_s[1].astype(f32) + fa_s[...].astype(f32)).astype(bf16)
-    start(fc)
-    project(me.x * 2 + far_c, put(proj_s.at[2]))
-    start(fb)
-    project(me.x * 2 + me.c, put(proj_s.at[3]))
+        read_s[j] = (normed * hg_ref[...].reshape(1, width) * open_gate).astype(bf16)
+
+    ro_no = [wire.slot() for _ in range(3)]
+    peers = [(far_x, far_c), (far_x, me.c), (me.x, far_c)]
+
+    def exchange(i):
+        x, c = peers[i]
+        return wire.copy(read_s.at[x * 2 + c], heads_s.at[me.tp], ro_no[i], me.at(x=x, c=c))
+
+    for i in range(3):
+        project(peers[i][0] * 2 + peers[i][1])
+        start(exchange(i))
+    project(me.tp)
+    relay_up(planes[1], 1)
+    relay_up(planes[2], 1)
+    who_wo = far_x * 2 + me.c
+    heads_row(wo_no[0], over, who_wo).wait_recv()
+    start(heads_row(wo_no[2], core, who_wo))
     res_in.wait()
-    fb.wait_recv()
-    near_sum = res_s[...].astype(f32) + proj_s[3].astype(f32) + fb_s[...].astype(f32)
-    mixed_s[...] = near_sum
-    fc.wait_recv()
-    mixed = mixed_s[...] + fc_in_s[...].astype(f32)
-    mixed_s[...] = mixed
+    wo_in.wait()
+
+    def head_part(rows_ref, owner_tp):
+        part = jnp.dot(rows_ref[...], wo_s[owner_tp], preferred_element_type=f32)
+        return part.astype(bf16).astype(f32)
+
+    mixed_s[...] = res_s[...].astype(f32) + head_part(read_s.at[me.tp], me.tp)
+    for i in (2, 1, 0):
+        x, c = peers[i]
+        frm = x * 2 + c
+        if i == 2:
+            heads_row(wo_no[1], core, frm).wait_recv()
+        if i == 0:
+            heads_row(wo_no[2], core, frm).wait_recv()
+        wire.copy(read_s.at[me.tp], heads_s.at[frm], ro_no[i], me.at(x=x, c=c)).wait_recv()
+        mixed_s[...] += head_part(heads_s.at[frm], frm)
+    mixed = mixed_s[...]
     factor = lax.rsqrt(jnp.mean(mixed * mixed, axis=1, keepdims=True) + eps)
     mine = me.zp * n_tp + me.tp
-    nrm_s[mine] = (mixed * factor * ng_ref[...]).astype(bf16)
+    nrm_s[mine] = (mixed * factor * ng_ref[...].reshape(1, nrm_s.shape[2])).astype(bf16)
+
+    inner = jnp.where(me.base == 0, 1, me.base)
+    others = [
+        jnp.where(me.base == 0, 2 + i, lax.rem(me.base + line - 1 - i, line))
+        for i in range(line - 2)
+    ]
+    course = [others[0], inner] + others[1:] + [2 * me.base + 1 - inner]
+    order = []
+    for z in course:
+        order += [(z, me.y), (z, 1 - me.y)]
+
+    def relay_dn(z, h, cond=None):
+        ref = dn_s.at[z * 2 + me.y, dn_part[h]]
+        got = wire.copy(ref, ref, dn_z[h] + z, me.at(z=z))
+        if cond is None:
+            got.wait_recv()
+        else:
+            pl.when(cond)(got.wait_recv)
+        start(over_dn(z, h), cond)
 
     def owner(zp, x, c):
         return zp * n_tp + x * 2 + c
 
     far_z = 1 - me.zp
-    n_core = [wire.slot() for _ in range(5)]
-    n_x, n_z, n_xh, n_zh = wire.slot(), wire.slot(), wire.slot(), wire.slot()
-    top_half, low_half = pl.ds(0, half), pl.ds(half, half)
+    n_core = [wire.slot() for _ in range(4)]
+    n_x, n_z, n_xh = wire.slot(), wire.slot(), wire.slot()
 
     def pass_on(number, where, who, part=None):
         ref = nrm_s.at[who] if part is None else nrm_s.at[who, part]
@@ -762,14 +816,12 @@
     start(pass_on(n_x, over, mine))
     start(pass_on(n_z, above, mine))
     start(pass_on(n_core[0], core, mine))
-    for i in range(2, line):
-        send_dn(i)
-    send_dn(1)
-    cross_dn(me.z, dn_piece(me.z))
-
-    up_in.wait()
-    for z in planes:
-        crossed_up(z)
+    send_dn(planes[2], 1)
+    for h in range(2):
+        for i in range(3, line):
+            send_dn(planes[i], h, inner_line)
+    for h in range(2):
+        start(over_dn(me.z, h, True))
 
     def raise_rows(zp, x):
         group = zp * 2 + x
@@ -784,77 +836,68 @@
 
         lax.fori_loop(0, hidden // 256, chunk, 0)
 
+    who = owner(me.zp, far_x, me.c)
+    pass_on(n_x, over, who).wait_recv()
+    start(pass_on(n_core[1], core, who))
+    near_dn = [send_dn(planes[1], h) for h in range(2)]
+    for h in range(2):
+        for i in range(3, line):
+            relay_up(planes[i], h)
+    relay_dn(planes[2], 0)
+    who = owner(far_z, me.x, me.c)
+    pass_on(n_z, above, who).wait_recv()
+    start(pass_on(n_xh, over, who))
+    start(pass_on(n_core[2], core, who))
+    for copy in own_in:
+        copy.wait()
+    for z in planes:
+        for h in range(2):
+            crossed_up(z, h)
     pass_on(n_core[0], core, owner(me.zp, me.x, far_c)).wait_recv()
     raise_rows(me.zp, me.x)
-    who = owner(me.zp, far_x, me.c)
-    pass_on(n_x, over, who).wait_recv()
-    start(pass_on(n_zh, above, who, top_half))
-    start(pass_on(n_core[1], core, who))
-    who = owner(far_z, me.x, me.c)
-    pass_on(n_z, above, who).wait_recv()
-    start(pass_on(n_xh, over, who, low_half))
-    start(pass_on(n_core[2], core, who))
     pass_on(n_core[1], core, owner(me.zp, far_x, far_c)).wait_recv()
     raise_rows(me.zp, far_x)
     pass_on(n_core[2], core, owner(far_z, me.x, far_c)).wait_recv()
     raise_rows(far_z, me.x)
+    relay_dn(planes[2], 1)
+    for h in range(2):
+        for i in range(3, line):
+            relay_dn(planes[i], h, inner_line)
     who = owner(far_z, far_x, me.c)
-    pass_on(n_zh, above, who, top_half).wait_recv()
-    start(pass_on(n_core[3], core, who, top_half))
-    pass_on(n_xh, over, who, low_half).wait_recv()
-    start(pass_on(n_core[4], core, who, low_half))
-    who = owner(far_z, far_x, far_c)
-    pass_on(n_core[3], core, who, top_half).wait_recv()
-    pass_on(n_core[4], core, who, low_half).wait_recv()
+    pass_on(n_xh, over, who).wait_recv()
+    start(pass_on(n_core[3], core, who))
+    pass_on(n_core[3], core, owner(far_z, far_x, far_c)).wait_recv()
+    for copy in near_dn:
+        drain(copy)
+    for h in range(2):
+        for i in range(3, line):
+            send_dn(planes[i], h, ends_line)
     raise_rows(far_z, far_x)
+    for copy in dn_in:
+        copy.wait()
 
     blocks = n_sp
-    order = []
-    for i in range(line):
-        z = lax.rem(me.base + i, line)
-        order += [(z, me.y), (z, 1 - me.y)]
     r1_no = [wire.slot() for _ in range(blocks)]
     r2_no = [wire.slot() for _ in range(blocks)]
     r3_no = [wire.slot() for _ in range(blocks)]
     groups = 4
 
-    def pump(i):
-        z = lax.rem(me.base + i, line)
-
-        @pl.when(z == me.z)
-        def _():
-            dn_in.wait()
-
-        if i < 2:
-
-            @pl.when(z != me.z)
-            def _():
-                recv_dn(z)
-                wire.copy(
-                    dn_s.at[z * 2 + me.y], dn_s.at[z * 2 + me.y], dn_y + z, me.at(y=1 - me.y)
-                ).start()
-
-            waits.append(
-                (
-                    wire.copy(
-                        dn_s.at[z * 2 + me.y], dn_s.at[z * 2 + me.y], dn_y + z, me.at(y=1 - me.y)
-                    ),
-                    z != me.z,
-                )
-            )
-        else:
-            recv_dn(z)
-            cross_dn(z)
-
     def lower(k):
         z, y = order[k]
-        if k % 2 == 0:
-            if k == 0:
-                pump(0)
-            if k // 2 + 1 < line:
-                pump(k // 2 + 1)
-        else:
-            crossed_dn(z)
+        if k == 0:
+            relay_dn(planes[1], 0, ends_line)
+        if k == 1:
+            relay_dn(planes[1], 1, ends_line)
+        if k == 3:
+            for h in range(2):
+                for i in range(3, line):
+                    relay_dn(planes[i], h, ends_line)
+        if k == 5:
+            for h in range(2):
+                relay_dn(planes[1], h, inner_line)
+        if k % 2 == 1:
+            for h in range(2):
+                crossed_dn(z, h)
         slot = z * 2 + y
 
         def one(g, carry):
@@ -873,41 +916,41 @@
             return part_s[k, me.c, g].astype(f32) + r1_s[k, g].astype(f32)
 
         for i in range(2):
-            away = i * 2 + far_x if k % 2 == 0 else far_z * 2 + i
+            away = i * 2 + far_x
             r2_out_s[k, i] = both(away).astype(bf16)
-        start(wire.copy(r2_out_s.at[k], r2_in_s.at[k], r2_no[k], over if k % 2 == 0 else above))
+        start(wire.copy(r2_out_s.at[k], r2_in_s.at[k], r2_no[k], over))
         for i in range(2):
-            here = i * 2 + me.x if k % 2 == 0 else me.zp * 2 + i
+            here = i * 2 + me.x
             r2_keep_s[k, i] = both(here)
 
     def sum2(k):
         wire.copy(
-            r2_out_s.at[k], r2_in_s.at[k], r2_no[k], over if k % 2 == 0 else above
+            r2_out_s.at[k], r2_in_s.at[k], r2_no[k], over
         ).wait_recv()
-        far = far_z if k % 2 == 0 else far_x
+        far = far_z
         r3_out_s[k] = (r2_keep_s[k, far] + r2_in_s[k, far].astype(f32)).astype(bf16)
-        start(wire.copy(r3_out_s.at[k], r3_in_s.at[k], r3_no[k], above if k % 2 == 0 else over))
+        start(wire.copy(r3_out_s.at[k], r3_in_s.at[k], r3_no[k], above))
 
     def sum3(k):
         wire.copy(
-            r3_out_s.at[k], r3_in_s.at[k], r3_no[k], above if k % 2 == 0 else over
+            r3_out_s.at[k], r3_in_s.at[k], r3_no[k], above
         ).wait_recv()
         z, y = order[k]
         c0 = pl.multiple_of((z * 2 + y) * wide, wide)
-        at = me.zp if k % 2 == 0 else me.x
+        at = me.zp
         total = r2_keep_s[k, at] + r2_in_s[k, at].astype(f32) + r3_in_s[k].astype(f32)
         total = mixed_s[:, pl.ds(c0, wide)] + total
         out_ref[:, pl.ds(c0, wide)] = total.astype(bf16)
 
-    for k in range(blocks + 3):
+    for k in range(blocks + 4):
         if k < blocks:
             lower(k)
         if 0 <= k - 1 < blocks:
             sum1(k - 1)
         if 0 <= k - 2 < blocks:
             sum2(k - 2)
-        if 0 <= k - 3 < blocks:
-            sum3(k - 3)
+        if 0 <= k - 4 < blocks:
+            sum3(k - 4)
 
     for copy, cond in waits:
         if cond is None:
@@ -939,14 +982,14 @@
     hidden = w_up.shape[1] // 2
     line = n_sp // 2
     blocks = n_sp
-    numbers = 4 * line + 24 + 3 * blocks
+    numbers = 8 * line + 27 + 3 * blocks
     vmem = pltpu.VMEM
     scratch = [
         vmem((length, depth), bf16),
         vmem((length, depth), bf16),
         vmem((length, width), bf16),
         vmem((length, width), bf16),
-        vmem((width, model), bf16),
+        vmem((n_tp, width, model), bf16),
         vmem((rows, model), bf16),
         vmem((n_sp, deep, hidden), bf16),
         vmem((n_sp, hidden, wide), bf16),
@@ -961,11 +1004,8 @@
         vmem((2, depth, width), bf16),
         vmem((2, 8, depth), f32),
         vmem((2, depth, width), bf16),
-        vmem((4, rows, model), bf16),
-        vmem((rows, model), bf16),
-        vmem((rows, model), bf16),
-        vmem((rows, model), bf16),
-        vmem((rows, model), bf16),
+        vmem((n_tp, rows, width), bf16),
+        vmem((n_tp, rows, width), bf16),
         vmem((rows, model), f32),
         vmem((2 * n_tp, rows, model), bf16),
         vmem((4, 2 * rows, hidden), bf16),
@@ -976,7 +1016,7 @@
         vmem((blocks, 2, rows, wide), bf16),
         vmem((blocks, rows, wide), bf16),
         vmem((blocks, rows, wide), bf16),
-        pltpu.SemaphoreType.DMA((8,)),
+        pltpu.SemaphoreType.DMA((10,)),
         pltpu.SemaphoreType.DMA((numbers,)),
         pltpu.SemaphoreType.DMA((numbers,)),
     ]
@@ -988,20 +1028,22 @@
         in_specs=[anywhere] * 4 + [inside] * 4 + [anywhere] * 2 + [inside] + [anywhere] * 2,
         out_specs=inside,
         scratch_shapes=scratch,
-        compiler_params=pltpu.CompilerParams(has_side_effects=True, vmem_limit_bytes=66_000_000),
+        compiler_params=pltpu.CompilerParams(
+            collective_id=0, has_side_effects=True, vmem_limit_bytes=66_000_000
+        ),
         name="layer",
     )(
         queries,
         keys,
         values,
         out_gate,
-        input_gates.reshape(2, length),
-        forget_gates.reshape(2, length),
-        doc_ids.reshape(1, length),
-        head_gain.reshape(1, width),
+        input_gates,
+        forget_gates,
+        doc_ids,
+        head_gain,
         w_out,
         resid,
-        norm_gain.reshape(1, model),
+        norm_gain,
         w_up,
         w_down,
     )

time: 225 us -> 161 us (0.72)
  Pallas kernels: 220 us -> 158 us
  local copies, waits for them, and re-layouts: 4.66 us -> 2.09 us
    pallas_call x1, Pallas kernels: 220 us -> 158 us  [fused(): pl.pallas_call(functools.partial(layer_kernel, n_sp, n_tp), out_shape=jax...]
where the time goes in v1:
time: 161 us; the launch traced here: 160 us
  Pallas kernels  158 us (98%)
  local copies, waits for them, and re-layouts  2.09 us (1%)
    pallas_call x1, Pallas kernels, fused(): pl.pallas_call(functools.partial(layer_kernel, n_sp, n_tp), out_shape=jax...  158 us

profile of v1, /device:TPU:0, one launch (start us, length us, event | category | flops | bytes accessed | tf_op | source)
XLA Modules:
  0.0 160.5 jit_solution(598621645378139110)
XLA Ops:
  0.0 158.4 %layer.1 = bf16[192,2048]{1,0:T(8,128)(2,1)} custom-call(bf16[768,256]{1,0:T(8,128)(2,1)} %q_hbm.1, bf16[768,256]{1,0:T(8,128)(2,1)} %k_hbm.1, bf16[768,512]{1,0:T(8,128)(2,1)} %v_hbm.1, bf16[768,512]{1,0:T(8,128)(2,1)} %og_hbm.1, f32[2,1,768]{2,1,0:T(1,128)} %ig_ref.1, f32[2,1,768]{2,1,0:T(1,128)} %fg_ref.1, s32[768]{0:T(1024)} %doc_ref.1, f32[512]{0:T(512)} %hg_ref.1, ...), custom_call_target="tpu_custom_call" | custom-call | tf_op jit(solution)/shard_map/layer/pallas_call | solution.py:1025
  158.4 2.1 %copy.15 = bf16[192,2048]{1,0:T(8,128)(2,1)} copy(bf16[192,2048]{1,0:T(8,128)(2,1)} %layer.1) | data formatting | bytes 1572864

commit v2 on v1

--- a/solution.py
+++ b/solution.py
@@ -788,7 +788,7 @@
         jnp.where(me.base == 0, 2 + i, lax.rem(me.base + line - 1 - i, line))
         for i in range(line - 2)
     ]
-    course = [others[0], inner] + others[1:] + [2 * me.base + 1 - inner]
+    course = [inner, 2 * me.base + 1 - inner] + others
     order = []
     for z in course:
         order += [(z, me.y), (z, 1 - me.y)]
@@ -806,22 +806,27 @@
         return zp * n_tp + x * 2 + c
 
     far_z = 1 - me.zp
-    n_core = [wire.slot() for _ in range(4)]
-    n_x, n_z, n_xh = wire.slot(), wire.slot(), wire.slot()
+    n_core = [wire.slot() for _ in range(2)]
+    n_x = wire.slot()
+    n_z, n_xz = [wire.slot(), wire.slot()], [wire.slot(), wire.slot()]
+    n_corez, n_corexz = [wire.slot(), wire.slot()], [wire.slot(), wire.slot()]
+    half = rows // 2
+    parts = [pl.ds(0, half), pl.ds(half, half)]
 
     def pass_on(number, where, who, part=None):
         ref = nrm_s.at[who] if part is None else nrm_s.at[who, part]
         return wire.copy(ref, ref, number, where)
 
     start(pass_on(n_x, over, mine))
-    start(pass_on(n_z, above, mine))
+    for h in range(2):
+        start(pass_on(n_z[h], above, mine, parts[h]))
     start(pass_on(n_core[0], core, mine))
-    send_dn(planes[2], 1)
+    near_dn = [send_dn(planes[1], h) for h in range(2)]
+    for h in range(2):
+        start(over_dn(me.z, h, True))
     for h in range(2):
         for i in range(3, line):
-            send_dn(planes[i], h, inner_line)
-    for h in range(2):
-        start(over_dn(me.z, h, True))
+            relay_up(planes[i], h)
 
     def raise_rows(zp, x):
         group = zp * 2 + x
@@ -839,15 +844,15 @@
     who = owner(me.zp, far_x, me.c)
     pass_on(n_x, over, who).wait_recv()
     start(pass_on(n_core[1], core, who))
-    near_dn = [send_dn(planes[1], h) for h in range(2)]
     for h in range(2):
         for i in range(3, line):
-            relay_up(planes[i], h)
+            send_dn(planes[i], h, inner_line)
     relay_dn(planes[2], 0)
     who = owner(far_z, me.x, me.c)
-    pass_on(n_z, above, who).wait_recv()
-    start(pass_on(n_xh, over, who))
-    start(pass_on(n_core[2], core, who))
+    for h in range(2):
+        pass_on(n_z[h], above, who, parts[h]).wait_recv()
+        start(pass_on(n_xz[h], over, who, parts[h]))
+        start(pass_on(n_corez[h], core, who, parts[h]))
     for copy in own_in:
         copy.wait()
     for z in planes:
@@ -857,21 +862,20 @@
     raise_rows(me.zp, me.x)
     pass_on(n_core[1], core, owner(me.zp, far_x, far_c)).wait_recv()
     raise_rows(me.zp, far_x)
-    pass_on(n_core[2], core, owner(far_z, me.x, far_c)).wait_recv()
+    for h in range(2):
+        pass_on(n_corez[h], core, owner(far_z, me.x, far_c), parts[h]).wait_recv()
     raise_rows(far_z, me.x)
-    relay_dn(planes[2], 1)
-    for h in range(2):
-        for i in range(3, line):
-            relay_dn(planes[i], h, inner_line)
-    who = owner(far_z, far_x, me.c)
-    pass_on(n_xh, over, who).wait_recv()
-    start(pass_on(n_core[3], core, who))
-    pass_on(n_core[3], core, owner(far_z, far_x, far_c)).wait_recv()
     for copy in near_dn:
         drain(copy)
+    send_dn(planes[2], 1)
     for h in range(2):
-        for i in range(3, line):
-            send_dn(planes[i], h, ends_line)
+        relay_dn(planes[1], h)
+    who = owner(far_z, far_x, me.c)
+    for h in range(2):
+        pass_on(n_xz[h], over, who, parts[h]).wait_recv()
+        start(pass_on(n_corexz[h], core, who, parts[h]))
+    for h in range(2):
+        pass_on(n_corexz[h], core, owner(far_z, far_x, far_c), parts[h]).wait_recv()
     raise_rows(far_z, far_x)
     for copy in dn_in:
         copy.wait()
@@ -885,16 +889,18 @@
     def lower(k):
         z, y = order[k]
         if k == 0:
-            relay_dn(planes[1], 0, ends_line)
-        if k == 1:
-            relay_dn(planes[1], 1, ends_line)
-        if k == 3:
             for h in range(2):
                 for i in range(3, line):
-                    relay_dn(planes[i], h, ends_line)
-        if k == 5:
+                    send_dn(planes[i], h, ends_line)
+        if k == 1:
             for h in range(2):
-                relay_dn(planes[1], h, inner_line)
+                for i in range(3, line):
+                    relay_dn(planes[i], h, inner_line)
+        if k == 3:
+            relay_dn(planes[2], 1)
+        if k in (4, 5):
+            for i in range(3, line):
+                relay_dn(planes[i], k - 4, ends_line)
         if k % 2 == 1:
             for h in range(2):
                 crossed_dn(z, h)
@@ -909,6 +915,9 @@
         lax.fori_loop(0, groups, one, 0)
         start(wire.copy(part_s.at[k, far_c], r1_s.at[k], r1_no[k], core))
 
+    def over_x(k):
+        return k < blocks // 2 or k % 2 == 1
+
     def sum1(k):
         wire.copy(part_s.at[k, far_c], r1_s.at[k], r1_no[k], core).wait_recv()
 
@@ -916,37 +925,35 @@
             return part_s[k, me.c, g].astype(f32) + r1_s[k, g].astype(f32)
 
         for i in range(2):
-            away = i * 2 + far_x
+            away = i * 2 + far_x if over_x(k) else far_z * 2 + i
             r2_out_s[k, i] = both(away).astype(bf16)
-        start(wire.copy(r2_out_s.at[k], r2_in_s.at[k], r2_no[k], over))
+        start(wire.copy(r2_out_s.at[k], r2_in_s.at[k], r2_no[k], over if over_x(k) else above))
         for i in range(2):
-            here = i * 2 + me.x
+            here = i * 2 + me.x if over_x(k) else me.zp * 2 + i
             r2_keep_s[k, i] = both(here)
 
     def sum2(k):
-        wire.copy(
-            r2_out_s.at[k], r2_in_s.at[k], r2_no[k], over
-        ).wait_recv()
-        far = far_z
+        first, second = (over, above) if over_x(k) else (above, over)
+        wire.copy(r2_out_s.at[k], r2_in_s.at[k], r2_no[k], first).wait_recv()
+        far = far_z if over_x(k) else far_x
         r3_out_s[k] = (r2_keep_s[k, far] + r2_in_s[k, far].astype(f32)).astype(bf16)
-        start(wire.copy(r3_out_s.at[k], r3_in_s.at[k], r3_no[k], above))
+        start(wire.copy(r3_out_s.at[k], r3_in_s.at[k], r3_no[k], second))
 
     def sum3(k):
-        wire.copy(
-            r3_out_s.at[k], r3_in_s.at[k], r3_no[k], above
-        ).wait_recv()
+        second = above if over_x(k) else over
+        wire.copy(r3_out_s.at[k], r3_in_s.at[k], r3_no[k], second).wait_recv()
         z, y = order[k]
         c0 = pl.multiple_of((z * 2 + y) * wide, wide)
-        at = me.zp
+        at = me.zp if over_x(k) else me.x
         total = r2_keep_s[k, at] + r2_in_s[k, at].astype(f32) + r3_in_s[k].astype(f32)
         total = mixed_s[:, pl.ds(c0, wide)] + total
         out_ref[:, pl.ds(c0, wide)] = total.astype(bf16)
 
     for k in range(blocks + 4):
+        if 0 <= k - 1 < blocks:
+            sum1(k - 1)
         if k < blocks:
             lower(k)
-        if 0 <= k - 1 < blocks:
-            sum1(k - 1)
         if 0 <= k - 2 < blocks:
             sum2(k - 2)
         if 0 <= k - 4 < blocks:
@@ -982,7 +989,7 @@
     hidden = w_up.shape[1] // 2
     line = n_sp // 2
     blocks = n_sp
-    numbers = 8 * line + 27 + 3 * blocks
+    numbers = 8 * line + 32 + 3 * blocks
     vmem = pltpu.VMEM
     scratch = [
         vmem((length, depth), bf16),

time: 161 us -> 152 us (0.944); the launches traced: 160 us -> 150 us
  Pallas kernels: 158 us -> 147 us
    pallas_call x1, Pallas kernels: 158 us -> 147 us  [fused(): pl.pallas_call(functools.partial(layer_kernel, n_sp, n_tp), out_shape=jax...]
where the time goes in v2:
time: 152 us; the launch traced here: 150 us
  Pallas kernels  147 us (97%)
  local copies, waits for them, and re-layouts  2.09 us (1%)
    pallas_call x1, Pallas kernels, fused(): pl.pallas_call(functools.partial(layer_kernel, n_sp, n_tp), out_shape=jax...  147 us

profile of v2, /device:TPU:0, one launch (start us, length us, event | category | flops | bytes accessed | tf_op | source)
XLA Modules:
  0.0 149.6 jit_solution(17947544444785445460)
XLA Ops:
  0.0 147.5 %layer.1 = bf16[192,2048]{1,0:T(8,128)(2,1)} custom-call(bf16[768,256]{1,0:T(8,128)(2,1)} %q_hbm.1, bf16[768,256]{1,0:T(8,128)(2,1)} %k_hbm.1, bf16[768,512]{1,0:T(8,128)(2,1)} %v_hbm.1, bf16[768,512]{1,0:T(8,128)(2,1)} %og_hbm.1, f32[2,1,768]{2,1,0:T(1,128)} %ig_ref.1, f32[2,1,768]{2,1,0:T(1,128)} %fg_ref.1, s32[768]{0:T(1024)} %doc_ref.1, f32[512]{0:T(512)} %hg_ref.1, ...), custom_call_target="tpu_custom_call" | custom-call | tf_op jit(solution)/shard_map/layer/pallas_call | solution.py:1032
  147.5 2.1 %copy.15 = bf16[192,2048]{1,0:T(8,128)(2,1)} copy(bf16[192,2048]{1,0:T(8,128)(2,1)} %layer.1) | data formatting | bytes 1572864

commit v3 on v2

--- a/solution.py
+++ b/solution.py
@@ -446,10 +446,6 @@
             pl.when(cond)(copy.start)
             waits.append((copy, cond))
 
-    def drain(copy):
-        copy.wait_send()
-        waits[:] = [item for item in waits if item[0] is not copy]
-
     def load(src, dst, number):
         copy = pltpu.make_async_copy(src, dst, local_sem.at[number])
         copy.start()
@@ -802,10 +798,51 @@
             pl.when(cond)(got.wait_recv)
         start(over_dn(z, h), cond)
 
+    blocks = n_sp
+    r1_no = [wire.slot() for _ in range(blocks)]
+    r2_no = [wire.slot() for _ in range(blocks)]
+    r3_no = [wire.slot() for _ in range(blocks)]
+    split = 4
+    r1_far = [wire.slot() for _ in range(split)][0]
+    r2_far = [wire.slot() for _ in range(split)][0]
+    r1_near, r2_near = r1_no[0], r2_no[0]
+    first_own = jnp.where(me.z == inner, 0, 2)
+    far_z = 1 - me.zp
+
+    def r1_part(k, zp, number):
+        pair = pl.ds(zp * 2, 2)
+        return wire.copy(part_s.at[k, far_c, pair], r1_s.at[k, pair], number + k, core)
+
+    def r2_part(k, zp, number):
+        return wire.copy(r2_out_s.at[k, zp], r2_in_s.at[k, zp], number + k, over)
+
+    def part_dot(k, slot, zp, number):
+        for x in range(2):
+            g = zp * 2 + x
+            value = jnp.dot(hid_s[g], dn_s[slot], preferred_element_type=f32).astype(bf16)
+            part_s[k, 0, g] = value[:rows]
+            part_s[k, 1, g] = value[rows:]
+        r1_part(k, zp, number).start()
+
+    def part_sum(k, zp, first, second):
+        r1_part(k, zp, first).wait_recv()
+
+        def both(g):
+            return part_s[k, me.c, g].astype(f32) + r1_s[k, g].astype(f32)
+
+        r2_out_s[k, zp] = both(zp * 2 + far_x).astype(bf16)
+        r2_part(k, zp, second).start()
+        r2_keep_s[k, zp] = both(zp * 2 + me.x)
+
+    for k in range(split):
+        waits.append((r1_part(k, me.zp, r1_near), None))
+        waits.append((r1_part(k, far_z, r1_far), None))
+        waits.append((r2_part(k, me.zp, r2_near), None))
+        waits.append((r2_part(k, far_z, r2_far), None))
+
     def owner(zp, x, c):
         return zp * n_tp + x * 2 + c
 
-    far_z = 1 - me.zp
     n_core = [wire.slot() for _ in range(2)]
     n_x = wire.slot()
     n_z, n_xz = [wire.slot(), wire.slot()], [wire.slot(), wire.slot()]
@@ -821,7 +858,8 @@
     for h in range(2):
         start(pass_on(n_z[h], above, mine, parts[h]))
     start(pass_on(n_core[0], core, mine))
-    near_dn = [send_dn(planes[1], h) for h in range(2)]
+    for h in range(2):
+        send_dn(planes[1], h)
     for h in range(2):
         start(over_dn(me.z, h, True))
     for h in range(2):
@@ -860,30 +898,30 @@
             crossed_up(z, h)
     pass_on(n_core[0], core, owner(me.zp, me.x, far_c)).wait_recv()
     raise_rows(me.zp, me.x)
+    send_dn(planes[2], 1)
     pass_on(n_core[1], core, owner(me.zp, far_x, far_c)).wait_recv()
     raise_rows(me.zp, far_x)
     for h in range(2):
         pass_on(n_corez[h], core, owner(far_z, me.x, far_c), parts[h]).wait_recv()
     raise_rows(far_z, me.x)
-    for copy in near_dn:
-        drain(copy)
-    send_dn(planes[2], 1)
     for h in range(2):
         relay_dn(planes[1], h)
+    for copy in dn_in:
+        copy.wait()
+    for h in range(2):
+        crossed_dn(me.z, h)
+    part_dot(first_own, me.sp, me.zp, r1_near)
+    part_dot(first_own + 1, me.z * 2 + 1 - me.y, me.zp, r1_near)
     who = owner(far_z, far_x, me.c)
     for h in range(2):
         pass_on(n_xz[h], over, who, parts[h]).wait_recv()
         start(pass_on(n_corexz[h], core, who, parts[h]))
     for h in range(2):
         pass_on(n_corexz[h], core, owner(far_z, far_x, far_c), parts[h]).wait_recv()
+    part_sum(first_own, me.zp, r1_near, r2_near)
+    part_sum(first_own + 1, me.zp, r1_near, r2_near)
     raise_rows(far_z, far_x)
-    for copy in dn_in:
-        copy.wait()
-
-    blocks = n_sp
-    r1_no = [wire.slot() for _ in range(blocks)]
-    r2_no = [wire.slot() for _ in range(blocks)]
-    r3_no = [wire.slot() for _ in range(blocks)]
+
     groups = 4
 
     def lower(k):
@@ -901,10 +939,21 @@
         if k in (4, 5):
             for i in range(3, line):
                 relay_dn(planes[i], k - 4, ends_line)
+        slot = z * 2 + y
+        if k < split:
+
+            @pl.when(z != me.z)
+            def _():
+                if k % 2 == 1:
+                    for h in range(2):
+                        crossed_dn(z, h)
+                part_dot(k, slot, me.zp, r1_near)
+
+            part_dot(k, slot, far_z, r1_far)
+            return
         if k % 2 == 1:
             for h in range(2):
                 crossed_dn(z, h)
-        slot = z * 2 + y
 
         def one(g, carry):
             value = jnp.dot(hid_s[g], dn_s[slot], preferred_element_type=f32).astype(bf16)
@@ -916,9 +965,17 @@
         start(wire.copy(part_s.at[k, far_c], r1_s.at[k], r1_no[k], core))
 
     def over_x(k):
-        return k < blocks // 2 or k % 2 == 1
+        return k < split or k % 2 == 1
 
     def sum1(k):
+        if k < split:
+
+            @pl.when(order[k][0] != me.z)
+            def _():
+                part_sum(k, me.zp, r1_near, r2_near)
+
+            part_sum(k, far_z, r1_far, r2_far)
+            return
         wire.copy(part_s.at[k, far_c], r1_s.at[k], r1_no[k], core).wait_recv()
 
         def both(g):
@@ -934,7 +991,11 @@
 
     def sum2(k):
         first, second = (over, above) if over_x(k) else (above, over)
-        wire.copy(r2_out_s.at[k], r2_in_s.at[k], r2_no[k], first).wait_recv()
+        if k < split:
+            r2_part(k, me.zp, r2_near).wait_recv()
+            r2_part(k, far_z, r2_far).wait_recv()
+        else:
+            wire.copy(r2_out_s.at[k], r2_in_s.at[k], r2_no[k], first).wait_recv()
         far = far_z if over_x(k) else far_x
         r3_out_s[k] = (r2_keep_s[k, far] + r2_in_s[k, far].astype(f32)).astype(bf16)
         start(wire.copy(r3_out_s.at[k], r3_in_s.at[k], r3_no[k], second))
@@ -989,7 +1050,7 @@
     hidden = w_up.shape[1] // 2
     line = n_sp // 2
     blocks = n_sp
-    numbers = 8 * line + 32 + 3 * blocks
+    numbers = 8 * line + 40 + 3 * blocks
     vmem = pltpu.VMEM
     scratch = [
         vmem((length, depth), bf16),

time: 152 us -> 148 us (0.974)
  Pallas kernels: 147 us -> 145 us
    pallas_call x1, Pallas kernels: 147 us -> 145 us  [fused(): pl.pallas_call(functools.partial(layer_kernel, n_sp, n_tp), out_shape=jax...]
where the time goes in v3:
time: 148 us; the launch traced here: 147 us
  Pallas kernels  145 us (98%)
  local copies, waits for them, and re-layouts  2.09 us (1%)
    pallas_call x1, Pallas kernels, fused(): pl.pallas_call(functools.partial(layer_kernel, n_sp, n_tp), out_shape=jax...  145 us

profile of v3, /device:TPU:0, one launch (start us, length us, event | category | flops | bytes accessed | tf_op | source)
XLA Modules:
  0.0 147.1 jit_solution(132104869797740412)
XLA Ops:
  0.0 145.0 %layer.1 = bf16[192,2048]{1,0:T(8,128)(2,1)} custom-call(bf16[768,256]{1,0:T(8,128)(2,1)} %q_hbm.1, bf16[768,256]{1,0:T(8,128)(2,1)} %k_hbm.1, bf16[768,512]{1,0:T(8,128)(2,1)} %v_hbm.1, bf16[768,512]{1,0:T(8,128)(2,1)} %og_hbm.1, f32[2,1,768]{2,1,0:T(1,128)} %ig_ref.1, f32[2,1,768]{2,1,0:T(1,128)} %fg_ref.1, s32[768]{0:T(1024)} %doc_ref.1, f32[512]{0:T(512)} %hg_ref.1, ...), custom_call_target="tpu_custom_call" | custom-call | tf_op jit(solution)/shard_map/layer/pallas_call | solution.py:1093
  145.0 2.1 %copy.15 = bf16[192,2048]{1,0:T(8,128)(2,1)} copy(bf16[192,2048]{1,0:T(8,128)(2,1)} %layer.1) | data formatting | bytes 1572864
